TPU v7x, 32 devices: a whole 2x2x4 slice. The times are simulated.
32 devices in a mesh: grp: 2 (over y), sp: 4 (over z), tp: 4 (over x, core).
Axes of the slice: x: 2, y: 2, z: 4, core: 2. Of those that a mesh axis runs over, the one named last changes fastest.
Arguments:
- queries: bfloat16 [4096, 1024], P(('grp', 'sp'), 'tp'), parts along dimension 0, may hold values from -6 to 6
- memory_keys: bfloat16 [4096, 1024], P(('grp', 'sp'), 'tp'), parts along dimension 0, may hold values from -6 to 6
- memory_values: bfloat16 [4096, 1024], P(('grp', 'sp'), 'tp'), parts along dimension 0, may hold values from -6 to 6
- output_preactivation: bfloat16 [4096, 1024], P(('grp', 'sp'), 'tp'), parts along dimension 0, may hold values from -12 to 12
- input_preactivation: float32 [8, 4096], P('tp', ('grp', 'sp')), parts along dimension 1, may hold values from -6 to 140
- forget_preactivation: float32 [8, 4096], P('tp', ('grp', 'sp')), parts along dimension 1, as said below
- extra_forget_terms: float32 [8, 4096], P('tp', ('grp', 'sp')), parts along dimension 1, may hold values from -1 to 0, as said below
- head_norm_gain: float32 [128], replicated, may hold values from 0.1 to 1.9
- output_projection_matrix: bfloat16 [1024, 2048], P('tp'), may hold values from -0.1875 to 0.1875
- residual: bfloat16 [4096, 2048], P(('grp', 'sp', 'tp')), parts along dimension 0, may hold values from -6 to 6
- feedforward_norm_gain: float32 [2048], replicated, may hold values from 0.1 to 1.9
- feedforward_up_matrix: bfloat16 [2048, 8192], P('sp', 'tp'), may hold values from -0.125 to 0.125
- feedforward_down_matrix: bfloat16 [8192, 2048], P('tp', 'sp'), may hold values from -0.0625 to 0.0625
Outputs:
- layer_out: bfloat16 [4096, 2048], P(('grp', 'sp', 'tp')), parts along dimension 0
There are 2 independent parts, one for each index of `grp`. A program takes and returns all parts, laid end to end along the dimension named above; an argument that names none is the same for every part. Nothing has to cross between parts.
Inputs may be any that keep to these rules, and one draw needn't show every extreme that they name: `forget_preactivation`: forget gate pre-activations. `extra_forget_terms`: extra log forget terms, zero at most positions.
All inputs are finite; a program needn't handle non-finite values.
Results may differ from a plain program's by a relative error of at most 0.018.
Values may be sent and summed in bfloat16 or wider, within the bound.
A program may use at most 64 MiB of HBM per device.

v0:
```python
import jax
import jax.numpy as jnp
from jax import lax
from jax.sharding import PartitionSpec as P

BLOCK = 128
neg_big = -1e30
norm_eps = 1e-06
highest = lax.Precision.HIGHEST


def entering(x, axis, combine, identity):
    length, position = (lax.axis_size(axis), lax.axis_index(axis))
    everything = jax.tree.map(lambda part: lax.all_gather(part, axis), x)
    start = jax.tree.map(
        lambda part, zero: jnp.broadcast_to(jnp.asarray(zero, part.dtype), part.shape), x, identity
    )

    def step(k, before):
        reached = k < position
        new = combine(before, jax.tree.map(lambda part: part[k], everything))
        return jax.tree.map(lambda a, b: jnp.where(reached, a, b), new, before)

    return lax.fori_loop(0, length, step, start)


def rms_norm(tensor, gain_vec):
    mean_sq = jnp.mean(tensor * tensor, axis=-1, keepdims=True)
    return tensor * lax.rsqrt(mean_sq + norm_eps) * gain_vec


def combine(earlier, later):
    total_e, max_e, memory_e = earlier
    total_l, max_l, memory_l = later
    carried = total_l + max_e
    new_max = jnp.maximum(carried, max_l)
    old_part = jnp.exp(carried - new_max)
    new_part = jnp.exp(max_l - new_max)
    return (
        total_e + total_l,
        new_max,
        old_part[..., None, None] * memory_e + new_part[..., None, None] * memory_l,
    )


def block_summary(key_blk, val_blk, gate_blk, decay_logarithm):
    block_total = decay_logarithm[..., -1]
    tail_log = block_total[..., None] - decay_logarithm + gate_blk
    tail_max = jnp.max(tail_log, axis=-1)
    weights = jnp.exp(tail_log - tail_max[..., None])
    memory = jnp.einsum("bhsv,bhsk->bhvk", weights[..., None] * val_blk, key_blk, precision=highest)
    return (block_total, tail_max, memory)


def shards(
    queries,
    memory_keys,
    memory_values,
    output_preactivation,
    input_preactivation,
    forget_preactivation,
    extra_forget_terms,
    head_norm_gain,
    output_projection_matrix,
    residual,
    feedforward_norm_gain,
    feedforward_up_matrix,
    feedforward_down_matrix,
):
    tok_count = queries.shape[0]
    head_count = input_preactivation.shape[0]
    head_dim = queries.shape[1] // head_count
    block_len = BLOCK
    block_count = tok_count // block_len

    def to_blocks(tensor):
        return (
            tensor.astype(jnp.float32)
            .reshape(block_count, block_len, head_count, head_dim)
            .transpose(0, 2, 1, 3)
        )

    def gate_block_list(tensor):
        return tensor.reshape(head_count, block_count, block_len).transpose(1, 0, 2)

    query_blk = to_blocks(queries)
    key_blk = to_blocks(memory_keys) * head_dim ** (-0.5)
    val_blk = to_blocks(memory_values)
    gate_blk = gate_block_list(input_preactivation)
    decay_logarithm = jnp.cumsum(
        gate_block_list(jax.nn.log_sigmoid(forget_preactivation) + extra_forget_terms), axis=-1
    )
    summaries = block_summary(key_blk, val_blk, gate_blk, decay_logarithm)
    zero_heads = jnp.zeros((head_count,), jnp.float32)
    zero_memory = jnp.zeros((head_count, head_dim, head_dim), jnp.float32)
    zero_state = (zero_heads, jnp.full((head_count,), neg_big, jnp.float32), zero_memory)
    prefixes = []
    running = zero_state
    for block_idx in range(block_count):
        prefixes.append(running)
        running = combine(running, tuple((member[block_idx] for member in summaries)))
    before = entering(running, "sp", combine, zero_state)
    anchor = (zero_heads, zero_heads, zero_memory)
    incoming = combine(anchor, before)
    starts = [combine(incoming, prefix) for prefix in prefixes]
    start_max = jnp.stack([each_state[1] for each_state in starts])
    start_memory = jnp.stack([each_state[2] for each_state in starts])
    causal = lax.broadcasted_iota(jnp.int32, (block_len, block_len), 0) >= lax.broadcasted_iota(
        jnp.int32, (block_len, block_len), 1
    )
    log_weight = (
        decay_logarithm[..., :, None] - decay_logarithm[..., None, :] + gate_blk[..., None, :]
    )
    log_weight = jnp.where(causal, log_weight, neg_big)
    carry_log = decay_logarithm + start_max[..., None]
    row_max = jnp.maximum(jnp.max(log_weight, axis=-1), carry_log)
    scores = jnp.einsum("bhtd,bhsd->bhts", query_blk, key_blk, precision=highest) * jnp.exp(
        log_weight - row_max[..., None]
    )
    carry_scale = jnp.exp(carry_log - row_max)
    hidden = jnp.einsum("bhts,bhsv->bhtv", scores, val_blk, precision=highest)
    hidden = hidden + carry_scale[..., None] * jnp.einsum(
        "bhvk,bhtk->bhtv", start_memory, query_blk, precision=highest
    )
    hidden = hidden.transpose(0, 2, 1, 3).reshape(tok_count, head_count, head_dim)
    gated = rms_norm(hidden, head_norm_gain) * jax.nn.sigmoid(
        output_preactivation.astype(jnp.float32).reshape(tok_count, head_count, head_dim)
    )
    mixed = gated.reshape(tok_count, head_count * head_dim).astype(jnp.bfloat16)
    branch = lax.psum_scatter(
        jnp.dot(mixed, output_projection_matrix, preferred_element_type=jnp.float32).astype(
            jnp.bfloat16
        ),
        "tp",
        scatter_dimension=0,
        tiled=True,
    ).astype(jnp.float32)
    mid_state = (residual.astype(jnp.float32) + branch).astype(jnp.bfloat16)
    normed = rms_norm(mid_state.astype(jnp.float32), feedforward_norm_gain).astype(jnp.bfloat16)
    normed_all = lax.all_gather(normed, "tp", axis=0, tiled=True)
    upward = jnp.dot(
        normed_all,
        lax.all_gather(feedforward_up_matrix, "sp", axis=0, tiled=True),
        preferred_element_type=jnp.float32,
    )
    active = jnp.square(jax.nn.relu(upward)).astype(jnp.bfloat16)
    mlp_terms = jnp.dot(
        active,
        lax.all_gather(feedforward_down_matrix, "sp", axis=1, tiled=True),
        preferred_element_type=jnp.float32,
    )
    mlp_sum = lax.psum_scatter(
        mlp_terms.astype(jnp.bfloat16), "tp", scatter_dimension=0, tiled=True
    ).astype(jnp.float32)
    return (mid_state.astype(jnp.float32) + mlp_sum).astype(jnp.bfloat16)


def solution(mesh):
    in_specs = (
        P(("grp", "sp"), "tp"),
        P(("grp", "sp"), "tp"),
        P(("grp", "sp"), "tp"),
        P(("grp", "sp"), "tp"),
        P("tp", ("grp", "sp")),
        P("tp", ("grp", "sp")),
        P("tp", ("grp", "sp")),
        P(),
        P("tp", None),
        P(("grp", "sp", "tp"), None),
        P(),
        P("sp", "tp"),
        P("tp", "sp"),
    )
    out_specs = P(("grp", "sp", "tp"), None)
    return jax.shard_map(shards, mesh=mesh, in_specs=in_specs, out_specs=out_specs, check_vma=False)
```

profile of v0, /device:TPU:0, one launch (start us, length us, event | category | flops | bytes accessed | tf_op | source)
XLA Modules:
  0.0 468.9 jit_solution(10719103995341335332)
XLA Ops:
  6.6 0.8 fusion.50
  7.4 1.2 reduce_window_sum.11
  8.7 0.2 slice_reduce_fusion.3
  9.1 0.9 fusion.65
  10.0 0.8 subtract_exponential_fusion.2
  10.8 12.6 %all-gather.1 = f32[4,1,2]{2,1,0:T(1,128)S(1)} all-gather(f32[1,1,2]{2,1,0:T(1,128)S(1)} %get-tuple-element.255), channel_id=1, replica_groups=mesh['grp'=2,'sp'=4,'tp'=4] {'sp'}, dimensions={0}, use_global_device_ids=true | all-gather | bytes 40 | tf_op jit(solution)/shard_map/all_gather | solution.py:14
  23.5 7.6 %all-gather = f32[4,1,2]{2,1,0:T(1,128)S(1)} all-gather(f32[1,1,2]{2,1,0:T(1,128)S(1)} %get-tuple-element.256), channel_id=1, replica_groups=mesh['grp'=2,'sp'=4,'tp'=4] {'sp'}, dimensions={0}, use_global_device_ids=true | all-gather | bytes 40 | tf_op jit(solution)/shard_map/all_gather | solution.py:14
  31.0 1.0 reshape.306
  32.2 1.0 convert_multiply_fusion.2
  33.2 0.3 mul.301
  33.5 0.7 fusion.22
  34.4 15.0 %all_gather.23 = f32[4,2,128,128]{3,2,1,0:T(8,128)S(1)} all-gather(f32[1,2,128,128]{3,2,1,0:T(8,128)S(1)} %fusion.40), channel_id=1, replica_groups=mesh['grp'=2,'sp'=4,'tp'=4] {'sp'}, dimensions={0}, use_global_device_ids=true | all-gather | bytes 655360 | tf_op jit(solution)/shard_map/all_gather | solution.py:14
  49.4 0.6 while.18
  50.1 0.4 fusion.27
  50.7 0.7 fusion.5
  51.7 0.7 fusion.7
  52.4 0.4 multiply_reduce_fusion
  53.0 0.3 copy.58
  53.3 0.6 mul.356
  53.9 2.1 convolution_convert_fusion
  56.1 31.6 %reduce-scatter.3.cloned.1.call-done = bf16[128,2048]{1,0:T(8,128)(2,1)} async-done(((bf16[512,2048]{1,0:T(8,128)(2,1)}), bf16[128,2048]{1,0:T(8,128)(2,1)}) %reduce-scatter.3.cloned.1.call-update) | async-done | bytes 524304 | tf_op jit(solution)/shard_map/reduce_scatter | solution.py:130
  87.6 1.3 fusion.8
  89.0 2.0 fusion.10
  91.1 0.7 all-gather.8.cloned.1.call-update
  91.8 0.5 all-gather.10.cloned.1.call-update
  92.3 0.2 reduce-scatter.5.cloned.1.call-start
  92.6 21.2 %all-gather.6.cloned.1.call-done = bf16[512,2048]{1,0:T(8,128)(2,1)} async-done(((bf16[128,2048]{1,0:T(8,128)(2,1)}), bf16[512,2048]{1,0:T(8,128)(2,1)}) %all-gather.6.cloned.1.call-update) | async-done | bytes 2097168 | tf_op jit(solution)/shard_map/all_gather | solution.py:140
  113.8 151.2 %all-gather.8.cloned.1.call-done = bf16[2048,2048]{1,0:T(8,128)(2,1)} async-done(((bf16[512,2048]{1,0:T(8,128)(2,1)}), bf16[2048,2048]{1,0:T(8,128)(2,1)}) %all-gather.8.cloned.1.call-update) | async-done | bytes 8388624 | tf_op jit(solution)/shard_map/all_gather | solution.py:143
  265.0 149.3 %all-gather.10.cloned.1.call-done = bf16[2048,2048]{1,0:T(8,128)(2,1)} async-done(((bf16[2048,512]{1,0:T(8,128)(2,1)}), bf16[2048,2048]{1,0:T(8,128)(2,1)}) %all-gather.10.cloned.1.call-update) | async-done | bytes 8388624 | tf_op jit(solution)/shard_map/all_gather | solution.py:149
  414.2 16.5 %convolution_convert_fusion.1 = bf16[512,2048]{1,0:T(8,128)(2,1)} fusion(bf16[2048,2048]{1,0:T(8,128)(2,1)} %all-gather.10.cloned.1.call-done, bf16[512,2048]{1,0:T(8,128)(2,1)} %all-gather.6.cloned.1.call-done, bf16[2048,2048]{1,0:T(8,128)(2,1)} %all-gather.8.cloned.1.call-done), kind=kOutput, calls=%fused_computation.16 | convolution fusion | flops 8594128896 | bytes 20971520 | tf_op jit(solution)/shard_map/dot_general | solution.py:147
  430.8 29.5 %reduce-scatter.5.cloned.1.call-done = bf16[128,2048]{1,0:T(8,128)(2,1)} async-done(((bf16[512,2048]{1,0:T(8,128)(2,1)}), bf16[128,2048]{1,0:T(8,128)(2,1)}) %reduce-scatter.5.cloned.1.call-update) | async-done | bytes 524304 | tf_op jit(solution)/shard_map/reduce_scatter | solution.py:152
  460.3 2.1 fusion.11
  (60 shorter events, 2.1 us)
Async XLA Ops:
  6.5 47.3 %copy-start = (bf16[256,2048]{1,0:T(8,128)(2,1)S(1)}, bf16[256,2048]{1,0:T(8,128)(2,1)}, u32[]{:S(2)}) copy-start(bf16[256,2048]{1,0:T(8,128)(2,1)} %param.23) | copy-start | bytes 3145732
  6.5 43.5 %copy-start.4 = (f32[2,512]{1,0:T(2,128)S(1)}, f32[2,512]{1,0:T(2,128)}, u32[]{:S(2)}) copy-start(f32[2,512]{1,0:T(2,128)} %param.19) | copy-start | bytes 12292
  6.5 44.1 %copy-start.7 = (f32[128]{0:T(128)S(1)}, f32[128]{0:T(128)}, u32[]{:S(2)}) copy-start(f32[128]{0:T(128)} %param.22) | copy-start | bytes 1540
  6.5 44.1 %copy-start.3 = (bf16[512,256]{1,0:T(8,128)(2,1)S(1)}, bf16[512,256]{1,0:T(8,128)(2,1)}, u32[]{:S(2)}) copy-start(bf16[512,256]{1,0:T(8,128)(2,1)} %param.15) | copy-start | bytes 786436
  6.5 81.1 %reduce-scatter.3.cloned.1.call-start = ((), (), s32[]{:S(2)}) async-start(), calls=%async_computation.2 | async-start | bytes 2621440 | tf_op jit(solution)/shard_map/reduce_scatter | solution.py:130
  50.7 3.2 copy-start.6
  53.0 34.7 %copy-start.1 = (bf16[128,2048]{1,0:T(8,128)(2,1)S(1)}, bf16[128,2048]{1,0:T(8,128)(2,1)}, u32[]{:S(2)}) copy-start(bf16[128,2048]{1,0:T(8,128)(2,1)} %param.24) | copy-start | bytes 1572868
  53.9 35.1 %copy-start.5 = (f32[2048]{0:T(1024)S(1)}, f32[2048]{0:T(1024)}, u32[]{:S(2)}) copy-start(f32[2048]{0:T(1024)} %param.25) | copy-start | bytes 24580
  56.0 57.7 %all-gather.6.cloned.1.call-start = ((), (), s32[]{:S(2)}) async-start(), calls=%async_computation.3 | async-start | bytes 2621440 | tf_op jit(solution)/shard_map/all_gather | solution.py:140
  91.0 174.0 %all-gather.8.cloned.1.call-start = ((), (), s32[]{:S(2)}) async-start(), calls=%async_computation.4 | async-start | bytes 10485760 | tf_op jit(solution)/shard_map/all_gather | solution.py:143
  91.8 322.5 %all-gather.10.cloned.1.call-start = ((), (), s32[]{:S(2)}) async-start(), calls=%async_computation.5 | async-start | bytes 10485760 | tf_op jit(solution)/shard_map/all_gather | solution.py:149
  92.3 368.0 %copy-start.2 = (bf16[128,2048]{1,0:T(8,128)(2,1)S(1)}, bf16[128,2048]{1,0:T(8,128)(2,1)}, u32[]{:S(2)}) copy-start(bf16[128,2048]{1,0:T(8,128)(2,1)} %reduce-scatter.3.cloned.1.call-done) | copy-start | bytes 1572868
  92.3 367.9 %reduce-scatter.5.cloned.1.call-start = ((), (), s32[]{:S(2)}) async-start(), calls=%async_computation.6 | async-start | bytes 2621440 | tf_op jit(solution)/shard_map/reduce_scatter | solution.py:152
Sparse Core Ops, SparseCore 0:
  56.1 31.4 reduce-scatter.2
  91.1 22.5 all-gather.5
  115.3 149.6 all-gather.7
  266.4 147.7 all-gather.9
  430.9 29.3 reduce-scatter.4
where the time goes:
time: 469 us
  waiting for transfers between devices  384 us (82%)
  blocking collectives  35.2 us (8%)
  matrix products  21.1 us (4%)
  between operations  13.4 us (3%)
  other arithmetic  11.6 us (2%)
    all_gather x1, waiting for transfers between devices, shards(): lax.all_gather(feedforward_up_matrix, 'sp', axis=0, tiled=True)  151 us
    all_gather x1, waiting for transfers between devices, shards(): lax.all_gather(feedforward_down_matrix, 'sp', axis=1, tiled=True)  149 us
    all_gather x3, blocking collectives, entering(): everything = jax.tree.map(lambda part: lax.all_gather(part, axis), x)  35.2 us
    reduce_scatter x1, waiting for transfers between devices, shards(): lax.psum_scatter(jnp.dot(mixed, output_projection_matrix, preferred_eleme...  31.6 us
    reduce_scatter x1, waiting for transfers between devices, shards(): lax.psum_scatter(mlp_terms.astype(jnp.bfloat16), 'tp', scatter_dimension=...  29.5 us
    all_gather x1, waiting for transfers between devices, shards(): normed_all = lax.all_gather(normed, 'tp', axis=0, tiled=True)  21.2 us
    dot_general x1, matrix products, shards(): jnp.dot(active, lax.all_gather(feedforward_down_matrix, 'sp', axis=1, til...  16.5 us
  transfers between devices with their start and end apart: 5, of which 5 were waited for; matrix products, arithmetic and copies ran while one was open for 0% of the time, Pallas kernels for 0%

commit v1 on v0

--- a/solution.py
+++ b/solution.py
@@ -144,10 +144,11 @@
         preferred_element_type=jnp.float32,
     )
     active = jnp.square(jax.nn.relu(upward)).astype(jnp.bfloat16)
+    raise_samples = lambda m, lane_axis: jnp.concatenate(
+        jax.lax.all_gather(m, axis_name=lane_axis), axis=1
+    )
     mlp_terms = jnp.dot(
-        active,
-        lax.all_gather(feedforward_down_matrix, "sp", axis=1, tiled=True),
-        preferred_element_type=jnp.float32,
+        active, raise_samples(feedforward_down_matrix, "sp"), preferred_element_type=jnp.float32
     )
     mlp_sum = lax.psum_scatter(
         mlp_terms.astype(jnp.bfloat16), "tp", scatter_dimension=0, tiled=True

time: 469 us -> 439 us (0.936)
  waiting for transfers between devices: 384 us -> 338 us
  local copies, waits for them, and re-layouts: 3.07 us -> 14.7 us
    all_gather x1, waiting for transfers between devices: 149 us -> 116 us  [shards(): jax.lax.all_gather(m, axis_name=lane_axis)]
    reshape x0 -> x1, local copies, waits for them, and re-layouts: none -> 11.6 us  [shards(): jnp.concatenate(jax.lax.all_gather(m, axis_name=lane_axis), axis=1)]
    all_gather x1, waiting for transfers between devices: 21.2 us -> 10.5 us  [shards(): normed_all = lax.all_gather(normed, 'tp', axis=0, tiled=True)]
  transfers between devices with their start and end apart: 5 -> 5, of which waited for: 5 -> 5; matrix products, arithmetic and copies ran while one was open for 0% -> 3% of each run, Pallas kernels for 0% -> 0%
where the time goes in v1:
time: 439 us; the launch traced here: 438 us
  waiting for transfers between devices  338 us (77%)
  blocking collectives  36.6 us (8%)
  matrix products  21.2 us (5%)
  between operations  15.3 us (3%)
  local copies, waits for them, and re-layouts  14.7 us (3%)
  other arithmetic  11.6 us (3%)
    all_gather x1, waiting for transfers between devices, shards(): lax.all_gather(feedforward_up_matrix, 'sp', axis=0, tiled=True)  151 us
    all_gather x1, waiting for transfers between devices, shards(): jax.lax.all_gather(m, axis_name=lane_axis)  116 us
    all_gather x3, blocking collectives, entering(): everything = jax.tree.map(lambda part: lax.all_gather(part, axis), x)  36.6 us
    reduce_scatter x1, waiting for transfers between devices, shards(): lax.psum_scatter(jnp.dot(mixed, output_projection_matrix, preferred_eleme...  30.3 us
    reduce_scatter x1, waiting for transfers between devices, shards(): lax.psum_scatter(mlp_terms.astype(jnp.bfloat16), 'tp', scatter_dimension=...  29.5 us
    dot_general x1, matrix products, shards(): jnp.dot(active, raise_samples(feedforward_down_matrix, 'sp'), preferred_e...  16.6 us
    reshape x1, local copies, waits for them, and re-layouts, shards(): jnp.concatenate(jax.lax.all_gather(m, axis_name=lane_axis), axis=1)  11.6 us
    all_gather x1, waiting for transfers between devices, shards(): normed_all = lax.all_gather(normed, 'tp', axis=0, tiled=True)  10.5 us
  transfers between devices with their start and end apart: 5, of which 5 were waited for; matrix products, arithmetic and copies ran while one was open for 3% of the time, Pallas kernels for 0%

profile of v1, /device:TPU:0, one launch (start us, length us, event | category | flops | bytes accessed | tf_op | source)
XLA Modules:
  0.0 438.3 jit_solution(4009372981847480919)
XLA Ops:
  7.4 0.8 fusion.50
  8.2 1.2 reduce_window_sum.11
  9.9 0.8 fusion.65
  10.8 0.8 subtract_exponential_fusion.2
  11.6 1.0 convert_multiply_fusion.2
  12.6 0.3 mul.301
  12.9 1.0 reshape.312
  14.1 0.7 fusion.22
  15.0 17.4 %all_gather.26 = f32[4,2,128,128]{3,2,1,0:T(8,128)S(1)} all-gather(f32[1,2,128,128]{3,2,1,0:T(8,128)S(1)} %fusion.40), channel_id=1, replica_groups=mesh['grp'=2,'sp'=4,'tp'=4] {'sp'}, dimensions={0}, use_global_device_ids=true | all-gather | bytes 655360 | tf_op jit(solution)/shard_map/all_gather | solution.py:14
  32.3 11.7 %all-gather.2 = f32[4,1,2]{2,1,0:T(1,128)S(1)} all-gather(f32[1,1,2]{2,1,0:T(1,128)S(1)} %get-tuple-element.263), channel_id=1, replica_groups=mesh['grp'=2,'sp'=4,'tp'=4] {'sp'}, dimensions={0}, use_global_device_ids=true | all-gather | bytes 40 | tf_op jit(solution)/shard_map/all_gather | solution.py:14
  44.0 7.6 %all-gather.1 = f32[4,1,2]{2,1,0:T(1,128)S(1)} all-gather(f32[1,1,2]{2,1,0:T(1,128)S(1)} %get-tuple-element.264), channel_id=1, replica_groups=mesh['grp'=2,'sp'=4,'tp'=4] {'sp'}, dimensions={0}, use_global_device_ids=true | all-gather | bytes 40 | tf_op jit(solution)/shard_map/all_gather | solution.py:14
  51.6 0.6 while.18
  52.3 0.4 fusion.27
  52.9 0.7 fusion.5
  53.9 0.7 fusion.7
  54.5 0.4 multiply_reduce_fusion
  55.2 0.3 copy.72
  55.4 0.6 mul.356
  56.1 2.1 convolution_convert_fusion
  58.3 0.5 all-gather.11.cloned.1.call-update
  58.9 30.3 %reduce-scatter.3.cloned.1.call-done = bf16[128,2048]{1,0:T(8,128)(2,1)} async-done(((bf16[512,2048]{1,0:T(8,128)(2,1)}), bf16[128,2048]{1,0:T(8,128)(2,1)}) %reduce-scatter.3.cloned.1.call-update) | async-done | bytes 524304 | tf_op jit(solution)/shard_map/reduce_scatter | solution.py:130
  89.2 1.3 fusion.8
  90.5 2.0 fusion.10
  92.6 0.5 all-gather.9.cloned.1.call-update
  93.2 0.2 reduce-scatter.5.cloned.1.call-start
  93.4 116.1 %all-gather.11.cloned.1.call-done = bf16[8192,512]{1,0:T(8,128)(2,1)} async-done(((bf16[2048,512]{1,0:T(8,128)(2,1)}), bf16[8192,512]{1,0:T(8,128)(2,1)}) %all-gather.11.cloned.1.call-update) | async-done | bytes 8388624 | tf_op jit(solution)/shard_map/all_gather | solution.py:148
  209.4 11.6 %copy.74 = bf16[2048,4,512]{0,2,1:T(8,128)(2,1)} copy(bf16[2048,4,512]{2,0,1:T(8,128)(2,1)} %bitcast.210) | data formatting | bytes 16777216 | tf_op jit(solution)/shard_map/reshape | solution.py:147
  221.0 10.5 %all-gather.7.cloned.1.call-done = bf16[512,2048]{1,0:T(8,128)(2,1)} async-done(((bf16[128,2048]{1,0:T(8,128)(2,1)}), bf16[512,2048]{1,0:T(8,128)(2,1)}) %all-gather.7.cloned.1.call-update) | async-done | bytes 2097168 | tf_op jit(solution)/shard_map/all_gather | solution.py:140
  231.5 150.9 %all-gather.9.cloned.1.call-done = bf16[2048,2048]{1,0:T(8,128)(2,1)} async-done(((bf16[512,2048]{1,0:T(8,128)(2,1)}), bf16[2048,2048]{1,0:T(8,128)(2,1)}) %all-gather.9.cloned.1.call-update) | async-done | bytes 8388624 | tf_op jit(solution)/shard_map/all_gather | solution.py:143
  382.5 16.6 %convolution_convert_fusion.1 = bf16[512,2048]{1,0:T(8,128)(2,1)} fusion(bf16[2048,2048]{0,1:T(8,128)(2,1)} %bitcast.211, bf16[512,2048]{1,0:T(8,128)(2,1)} %all-gather.7.cloned.1.call-done, bf16[2048,2048]{1,0:T(8,128)(2,1)} %all-gather.9.cloned.1.call-done), kind=kOutput, calls=%fused_computation.16 | convolution fusion | flops 8594128896 | bytes 20971520 | tf_op jit(solution)/shard_map/dot_general | solution.py:150
  399.1 29.5 %reduce-scatter.5.cloned.1.call-done = bf16[128,2048]{1,0:T(8,128)(2,1)} async-done(((bf16[512,2048]{1,0:T(8,128)(2,1)}), bf16[128,2048]{1,0:T(8,128)(2,1)}) %reduce-scatter.5.cloned.1.call-update) | async-done | bytes 524304 | tf_op jit(solution)/shard_map/reduce_scatter | solution.py:153
  428.6 2.1 fusion.11
  (61 shorter events, 2.3 us)
Async XLA Ops:
  7.4 48.7 %copy-start = (bf16[256,2048]{1,0:T(8,128)(2,1)S(1)}, bf16[256,2048]{1,0:T(8,128)(2,1)}, u32[]{:S(2)}) copy-start(bf16[256,2048]{1,0:T(8,128)(2,1)} %param.23) | copy-start | bytes 3145732
  7.4 44.9 %copy-start.4 = (f32[2,512]{1,0:T(2,128)S(1)}, f32[2,512]{1,0:T(2,128)}, u32[]{:S(2)}) copy-start(f32[2,512]{1,0:T(2,128)} %param.19) | copy-start | bytes 12292
  7.4 45.4 %copy-start.3 = (bf16[512,256]{1,0:T(8,128)(2,1)S(1)}, bf16[512,256]{1,0:T(8,128)(2,1)}, u32[]{:S(2)}) copy-start(bf16[512,256]{1,0:T(8,128)(2,1)} %param.15) | copy-start | bytes 786436
  7.4 81.8 %reduce-scatter.3.cloned.1.call-start = ((), (), s32[]{:S(2)}) async-start(), calls=%async_computation.2 | async-start | bytes 2621440 | tf_op jit(solution)/shard_map/reduce_scatter | solution.py:130
  52.2 3.2 copy-start.7
  52.9 3.2 copy-start.6
  56.1 33.1 %copy-start.1 = (bf16[128,2048]{1,0:T(8,128)(2,1)S(1)}, bf16[128,2048]{1,0:T(8,128)(2,1)}, u32[]{:S(2)}) copy-start(bf16[128,2048]{1,0:T(8,128)(2,1)} %param.24) | copy-start | bytes 1572868
  56.1 34.4 %copy-start.5 = (f32[2048]{0:T(1024)S(1)}, f32[2048]{0:T(1024)}, u32[]{:S(2)}) copy-start(f32[2048]{0:T(1024)} %param.25) | copy-start | bytes 24580
  58.2 151.2 %all-gather.11.cloned.1.call-start = ((), (), s32[]{:S(2)}) async-start(), calls=%async_computation.6 | async-start | bytes 10485760 | tf_op jit(solution)/shard_map/all_gather | solution.py:148
  58.8 172.7 %all-gather.7.cloned.1.call-start = ((), (), s32[]{:S(2)}) async-start(), calls=%async_computation.3 | async-start | bytes 2621440 | tf_op jit(solution)/shard_map/all_gather | solution.py:140
  92.6 289.9 %all-gather.9.cloned.1.call-start = ((), (), s32[]{:S(2)}) async-start(), calls=%async_computation.4 | async-start | bytes 10485760 | tf_op jit(solution)/shard_map/all_gather | solution.py:143
  93.2 335.4 %reduce-scatter.5.cloned.1.call-start = ((), (), s32[]{:S(2)}) async-start(), calls=%async_computation.5 | async-start | bytes 2621440 | tf_op jit(solution)/shard_map/reduce_scatter | solution.py:153
  382.5 46.1 %copy-start.2 = (bf16[128,2048]{1,0:T(8,128)(2,1)S(1)}, bf16[128,2048]{1,0:T(8,128)(2,1)}, u32[]{:S(2)}) copy-start(bf16[128,2048]{1,0:T(8,128)(2,1)} %reduce-scatter.3.cloned.1.call-done) | copy-start | bytes 1572868
Sparse Core Ops, SparseCore 0:
  58.3 30.8 reduce-scatter.2
  399.2 29.3 reduce-scatter.4
Sparse Core Ops, SparseCore 1:
  60.3 149.1 all-gather.10
  210.9 20.6 all-gather.6
  233.0 149.5 all-gather.8
